TPU v7x, 256 devices: a whole 4x4x8 slice. The times are simulated.
256 devices in a mesh: sp: 64 (over z, x, core), tp: 4 (over y).
Axes of the slice: x: 4, y: 4, z: 8, core: 2. Of those that a mesh axis runs over, the one named last changes fastest.
Arguments:
- query_logits: bfloat16 [32768, 4096], P('sp', 'tp'), may hold values from -6 to 6
- forget_logits: bfloat16 [32768, 4096], P('sp', 'tp'), may hold values from -6 to 6
- value_inputs: bfloat16 [32768, 4096], P('sp', 'tp'), may hold values from -16 to 16
- output_gate_logits: bfloat16 [32768, 4096], P('sp', 'tp'), may hold values from -6 to 6
- forget_floor_gap: float32 [4096], replicated, may hold values from 3.0517578e-06 to 0.1
- surge_log_decay: float32 [32, 32768], P('tp', 'sp'), may hold values from -0.7 to 0
- head_norm_gain: float32 [128], replicated, may hold values from 0.1 to 1.9
- output_matrix: bfloat16 [4096, 4096], P('sp', 'tp'), may hold values from -1.25 to 1.25
- branch_norm_gain: float32 [4096], replicated, may hold values from 0.1 to 1.9
- residual: bfloat16 [32768, 4096], P('sp', 'tp'), may hold values from -6 to 6
Outputs:
- output: bfloat16 [32768, 4096], P('sp', 'tp')
All inputs are finite; a program needn't handle non-finite values.
Results may differ from a plain program's by a relative error of at most 0.005.
Values may be sent and summed in bfloat16 or wider, within the bound.
A program may use at most 128 MiB of HBM per device.

v0:
```python
import jax
import jax.numpy as jnp
from jax import lax
from jax.sharding import Mesh
from jax.sharding import PartitionSpec as P

HEAD_DIM = 128
D = 4096
BLOCK_SPAN = 64
SP = ("sp_0", "sp_1", "sp_2")


epsilon = 1e-06


def filled_with(shard, identity):
    return jax.tree.map(
        lambda a, e: jnp.broadcast_to(jnp.asarray(e, a.dtype), a.shape), shard, identity
    )


def carried_in(shard, axes, combine, identity):
    before = start = filled_with(shard, identity)
    so_far = shard
    for axis in reversed(axes):
        size, position = (lax.axis_size(axis), lax.axis_index(axis))
        pieces = jax.tree.map(lambda part: lax.all_gather(part, axis), so_far)
        inside, so_far = (start, start)
        for k in range(size):
            passed = k < position
            so_far = combine(so_far, jax.tree.map(lambda part: part[k], pieces))
            inside = jax.tree.map(lambda new, old: jnp.where(passed, new, old), so_far, inside)
        before = combine(inside, before)
    return before


def joined_along(tiles, dim):
    lengths = list(tiles.shape[1:])
    lengths[dim] *= tiles.shape[0]
    return jnp.moveaxis(tiles, 0, dim).reshape(lengths)


def gather_in_order(shard, axes, turns):
    tiles = shard[None]
    for k in turns:
        tiles = lax.all_gather(tiles, axes[k], axis=0, tiled=True)
    held = [lax.axis_size(axes[k]) for k in reversed(turns)]
    tiles = tiles.reshape(*held, *shard.shape)
    turned = sorted(range(len(turns)), key=lambda place: turns[len(turns) - 1 - place])
    return tiles.transpose(*turned, *range(len(turns), tiles.ndim)).reshape(-1, *shard.shape)


def whole_of(shard, axes, turns, dim):
    return joined_along(gather_in_order(shard, axes, turns), dim)


def block_update(state, queries, keys_in, values_in, running):
    length = running.shape[1]
    middle = length // 2
    anchor = running[:, middle - 1 : middle, :]
    ending = running[:, -1:, :]
    causal = jnp.tril(jnp.ones((length, length), dtype=bool))
    highest = lax.Precision.HIGHEST
    inter = jnp.einsum("htd,hde->hte", queries * jnp.exp(running), state, precision=highest)
    scores = jnp.einsum(
        "htd,hsd->hts",
        queries * jnp.exp(running - anchor),
        keys_in * jnp.exp(anchor - running),
        precision=highest,
    )
    intra = jnp.einsum(
        "hts,hse->hte", jnp.where(causal[None], scores, 0.0), values_in, precision=highest
    )
    new_state = state * jnp.exp(ending[:, 0, :])[:, :, None] + jnp.einsum(
        "hsd,hse->hde", keys_in * jnp.exp(ending - running), values_in, precision=highest
    )
    return (new_state, inter + intra)


def head_gates(query_logits, forget_logits, value_inputs, gap):
    row_count = query_logits.shape[0]
    head_count = query_logits.shape[1] // HEAD_DIM

    def shaped(array):
        return array.astype(jnp.float32).reshape(row_count, head_count, HEAD_DIM)

    queries = jax.nn.silu(shaped(query_logits)) * HEAD_DIM ** (-0.5)
    keys_in = gap.reshape(head_count, HEAD_DIM) * jax.nn.sigmoid(-shaped(forget_logits))
    values_in = shaped(value_inputs)
    decay_factors = jnp.log1p(-keys_in)
    return (queries, keys_in, values_in, decay_factors)


def gated_norm(heads_out, output_gate_logits, head_norm_gain):
    mean_sq = jnp.mean(heads_out * heads_out, axis=-1, keepdims=True)
    gates = jax.nn.silu(output_gate_logits.astype(jnp.float32).reshape(heads_out.shape))
    normed = heads_out * lax.rsqrt(mean_sq + epsilon) * head_norm_gain * gates
    return normed.reshape(heads_out.shape[0], -1).astype(jnp.bfloat16)


def combine(earlier, later):
    return (earlier[0] * later[0], later[0][:, :, None] * earlier[1] + later[1])


def per_device(
    query_logits,
    forget_logits,
    value_inputs,
    output_gate_logits,
    forget_floor_gap,
    surge_log_decay,
    head_norm_gain,
    output_matrix,
    branch_norm_gain,
    residual,
):
    row_count = query_logits.shape[0]
    head_cols = query_logits.shape[1]
    head_count = head_cols // HEAD_DIM
    number_of_blocks = row_count // BLOCK_SPAN
    column = lax.axis_index("tp")
    gap = lax.dynamic_slice_in_dim(forget_floor_gap, column * head_cols, head_cols)
    queries, keys_in, values_in, decay_factors = head_gates(
        query_logits, forget_logits, value_inputs, gap
    )
    decay_factors = decay_factors + jnp.transpose(surge_log_decay)[:, :, None]

    def to_blocks(array):
        return array.reshape(number_of_blocks, BLOCK_SPAN, head_count, HEAD_DIM).transpose(
            0, 2, 1, 3
        )

    queries = to_blocks(queries)
    running = jnp.cumsum(to_blocks(decay_factors), axis=2)

    def step_forward(state, input_tuple):
        return block_update(state, input_tuple[0], input_tuple[1], input_tuple[2], input_tuple[3])

    starting_state = jnp.zeros((head_count, HEAD_DIM, HEAD_DIM), jnp.float32)
    end_state, local_out = lax.scan(
        step_forward, starting_state, (queries, to_blocks(keys_in), to_blocks(values_in), running)
    )
    totals = running[:, :, -1, :]
    before = jnp.cumsum(totals, axis=0) - totals
    whole_decay = jnp.exp(jnp.sum(totals, axis=0))
    identity = (jnp.ones_like(whole_decay), jnp.zeros_like(end_state))
    unused_slot, carried = carried_in((whole_decay, end_state), SP, combine, identity)
    reach = queries * jnp.exp(running + before[:, :, None, :])
    heads_out = local_out + jnp.einsum(
        "nhtd,hde->nhte", reach, carried, precision=lax.Precision.HIGHEST
    )
    heads_out = heads_out.transpose(0, 2, 1, 3).reshape(row_count, head_count, HEAD_DIM)
    mixed_rows = gated_norm(heads_out, output_gate_logits, head_norm_gain)
    all_heads = lax.all_gather(mixed_rows, "tp", axis=1, tiled=True)
    projected = jnp.dot(
        all_heads, whole_of(output_matrix, SP, (1, 0, 2), 0), preferred_element_type=jnp.float32
    )
    branch = lax.optimization_barrier(projected.astype(jnp.bfloat16)).astype(jnp.float32)
    squares = lax.psum(jnp.sum(branch * branch, axis=1), "tp")
    scale = lax.rsqrt(squares / D + epsilon)
    out_cols = branch.shape[1]
    gain_part = lax.dynamic_slice_in_dim(branch_norm_gain, column * out_cols, out_cols)
    return (residual.astype(jnp.float32) + branch * scale[:, None] * gain_part).astype(jnp.bfloat16)


def solution(mesh):
    torus = Mesh(mesh.devices.reshape(8, 4, 2, mesh.shape["tp"]), ("sp_0", "sp_1", "sp_2", "tp"))
    in_specs = (
        P(SP, "tp"),
        P(SP, "tp"),
        P(SP, "tp"),
        P(SP, "tp"),
        P(),
        P("tp", SP),
        P(),
        P(SP, "tp"),
        P(),
        P(SP, "tp"),
    )
    out_specs = P(SP, "tp")
    return jax.shard_map(
        per_device, mesh=torus, in_specs=in_specs, out_specs=out_specs, check_vma=False
    )
```

profile of v0, /device:TPU:1, one launch (start us, length us, event | category | flops | bytes accessed | tf_op | source)
XLA Modules:
  0.0 339.1 jit_solution(1306000808769701150)
XLA Ops:
  6.5 1.8 divide_bitcast_fusion
  8.4 1.8 copy.58
  12.5 1.5 bitcast_bitcast_fusion
  14.0 3.9 %fusion.35 = f32[8,8,64,128]{3,1,2,0:T(8,128)} fusion(f32[8,64,8]{2,1,0:T(8,128)S(1)} %bitcast.317, f32[8,128]{1,0:T(8,128)S(1)} %dynamic-slice_bitcast_fusion, f32[8,64,8,128]{3,2,1,0:T(8,128)} %bitcast.308), kind=kOutput, calls=%fused_computation.57 | output fusion | flops 34603008 | bytes 4214784 | tf_op jit(solution)/shard_map/jit(cumsum)/reduce_window_sum | solution.py:134
  18.0 2.6 fusion.33
  20.5 47.0 %while.13 = (s32[]{:T(128)}, f32[8,128,128]{2,1,0:T(8,128)S(1)}, f32[8,8,64,128]{3,2,0,1:T(8,128)}, f32[8,8,64,128]{3,1,2,0:T(8,128)}, f32[8,8,64,128]{3,1,2,0:T...) while((s32[]{:T(128)}, f32[8,128,128]{2,1,0:T(8,128)S(1)}, ...), condition=%wide.region_2.3_spmd.clone, body=%wide.region_1.2_spmd.clone.sunk | while | flops 303075328 | bytes 7647856 | solution.py:140
  25.2 1.2 convolution_add_fusion.3
  31.1 1.2 convolution_add_fusion.3
  37.0 1.2 convolution_add_fusion.3
  42.9 1.2 convolution_add_fusion.3
  48.7 1.2 convolution_add_fusion.3
  54.6 1.2 convolution_add_fusion.3
  69.2 4.7 %all-gather = f32[16,128]{1,0:T(8,128)S(1)} all-gather(f32[8,128]{1,0:T(8,128)S(1)} %exp.52), channel_id=2, replica_groups=mesh['sp_0'=8,'sp_1'=4,'sp_2'=2,'tp'=4] {'sp_2'}, dimensions={0}, use_global_device_ids=true | all-gather | bytes 12288 | tf_op jit(solution)/shard_map/all_gather | solution.py:27
  73.8 13.5 %all-gather.21.cloned.1.call-done = f32[16,128,128]{2,1,0:T(8,128)} async-done(((f32[8,128,128]{2,1,0:T(8,128)}), f32[16,128,128]{2,1,0:T(8,128)}) %all-gather.21.cloned.1.call-update) | async-done | bytes 1048592 | tf_op jit(solution)/shard_map/all_gather | solution.py:27
  87.4 2.3 bitcast_add_fusion.5
  89.8 11.0 %all-gather.2 = bf16[256,1024]{1,0:T(8,128)(2,1)} all-gather(bf16[64,1024]{1,0:T(8,128)(2,1)S(1)} %copy-done.11), channel_id=4, replica_groups=mesh['sp_0'=8,'sp_1'=4,'sp_2'=2,'tp'=4] {'sp_1'}, dimensions={0}, use_global_device_ids=true | all-gather | bytes 655360 | tf_op jit(solution)/shard_map/all_gather | solution.py:46
  100.9 9.8 %all-gather.3 = f32[32,128]{1,0:T(8,128)S(1)} all-gather(f32[8,128]{1,0:T(8,128)S(1)} %get-tuple-element.133), channel_id=5, replica_groups=mesh['sp_0'=8,'sp_1'=4,'sp_2'=2,'tp'=4] {'sp_1'}, dimensions={0}, use_global_device_ids=true | all-gather | bytes 20480 | tf_op jit(solution)/shard_map/all_gather | solution.py:27
  110.7 13.0 %all-gather.11.cloned.1.call-done = f32[4,8,128,128]{3,2,1,0:T(8,128)} async-done(((f32[1,8,128,128]{3,2,1,0:T(8,128)}), f32[4,8,128,128]{3,2,1,0:T(8,128)}) %all-gather.11.cloned.1.call-update) | async-done | bytes 2097168 | tf_op jit(solution)/shard_map/all_gather | solution.py:27
  123.7 2.6 multiply_add_fusion
  126.4 54.0 %all-gather.17.cloned.1.call-done = bf16[32,64,1024]{2,1,0:T(8,128)(2,1)} async-done(((bf16[4,64,1024]{2,1,0:T(8,128)(2,1)}), bf16[32,64,1024]{2,1,0:T(8,128)(2,1)}) %all-gather.17.cloned.1.call-update) | async-done | bytes 4194320 | tf_op jit(solution)/shard_map/all_gather | solution.py:46
  180.4 19.6 %all_gather.40 = f32[8,8,128]{2,1,0:T(8,128)S(1)} all-gather(f32[1,8,128]{2,1,0:T(8,128)S(1)} %get-tuple-element.127), channel_id=1, replica_groups=mesh['sp_0'=8,'sp_1'=4,'sp_2'=2,'tp'=4] {'sp_0'}, dimensions={0}, use_global_device_ids=true | all-gather | bytes 36864 | tf_op jit(solution)/shard_map/all_gather | solution.py:27
  201.0 3.8 %exponential_multiply_fusion = f32[8,8,64,128]{3,1,2,0:T(8,128)} fusion(f32[8,8,64,128]{3,1,2,0:T(8,128)} %get-tuple-element.230, f32[8,8,128]{2,1,0:T(8,128)S(1)} %fusion.46, f32[8,64,8,128]{3,2,1,0:T(8,128)S(1)} %bitcast.307), kind=kLoop, calls=%fused_computation.64 | loop fusion | flops 3670016 | bytes 6324224 | tf_op jit(solution)/shard_map/mul | solution.py:148
  204.8 30.7 %all-gather.13.cloned.1.call-done = f32[8,8,128,128]{3,2,1,0:T(8,128)} async-done(((f32[1,8,128,128]{3,2,1,0:T(8,128)}), f32[8,8,128,128]{3,2,1,0:T(8,128)}) %all-gather.13.cloned.1.call-update) | async-done | bytes 4194320 | tf_op jit(solution)/shard_map/all_gather | solution.py:27
  235.5 8.2 %multiply_reduce_fusion = (f32[8,64,8]{1,0,2:T(8,128)S(1)}, f32[8,64,8,128]{3,1,0,2:T(8,128)S(1)}) fusion(f32[8,8,64,128]{3,2,0,1:T(8,128)} %get-tuple-element.43, f32[8,8,64,128]{3,1,2,0:T(8,128)} %exponential_multiply_fusion, f32[8,8,128,128]{3,2,1,0:T(8,128)} %all-gather.13.cloned.1.call-done, f32[4,8,128,128]{3,2,1,0:T(8,128)} %all-gather.11.cloned.1.call-done, ...), kind=kOutput, calls=%fused_computation.63 | convolution fusion | flops 812511232 | bytes 13713422 | tf_op jit(solution)/shard_map/nhtd,hde->nhte/dot_general | solution.py:149
  243.8 1.2 copy.41
  246.3 2.2 fusion.42
  248.5 13.3 %all-gather.19.cloned.1.call-done = bf16[64,64,1024]{2,1,0:T(8,128)(2,1)} async-done(((bf16[32,64,1024]{2,1,0:T(8,128)(2,1)}), bf16[64,64,1024]{2,1,0:T(8,128)(2,1)}) %all-gather.19.cloned.1.call-update) | async-done | bytes 8388624 | tf_op jit(solution)/shard_map/all_gather | solution.py:46
  261.9 8.4 %copy.43 = bf16[8,4,2,64,1024]{4,3,2,1,0:T(8,128)(2,1)} copy(bf16[8,4,2,64,1024]{4,3,1,0,2:T(8,128)(2,1)} %bitcast.310) | data formatting | bytes 16777216 | tf_op jit(solution)/shard_map/transpose | solution.py:50
  270.3 44.5 %all-gather.15.cloned.1.call-done = bf16[512,4096]{1,0:T(8,128)(2,1)} async-done(((bf16[512,1024]{1,0:T(8,128)(2,1)}), bf16[512,4096]{1,0:T(8,128)(2,1)}) %all-gather.15.cloned.1.call-update) | async-done | bytes 4194320 | tf_op jit(solution)/shard_map/all_gather | solution.py:154
  314.7 9.2 %convolution_convert_fusion = bf16[512,1024]{1,0:T(8,128)(2,1)S(1)} fusion(bf16[512,4096]{1,0:T(8,128)(2,1)} %all-gather.15.cloned.1.call-done, bf16[4096,1024]{1,0:T(8,128)(2,1)} %bitcast.311), kind=kOutput, calls=%fused_computation.71 | convolution fusion | flops 4295491584 | bytes 13631488 | tf_op jit(solution)/shard_map/dot_general | solution.py:155
  324.2 6.6 %psum.7 = f32[512]{0:T(512)S(1)} all-reduce(f32[512]{0:T(512)S(1)} %fusion.24), channel_id=1, replica_groups=mesh['sp_0'=8,'sp_1'=4,'sp_2'=2,'tp'=4] {'tp'}, use_global_device_ids=true, to_apply=%region_7.8 | all-reduce | flops 512 | bytes 4096 | tf_op jit(solution)/shard_map/psum | solution.py:159
  330.8 1.4 fusion.27
  (137 shorter events, 46.2 us)
Async XLA Ops:
  6.5 7.5 %copy-start = (f32[4096]{0:T(1024)S(1)}, f32[4096]{0:T(1024)}, u32[]{:S(2)}) copy-start(f32[4096]{0:T(1024)} %param.16) | copy-start | bytes 49156
  6.5 80.8 %all-gather.21.cloned.1.call-start = ((), (), s32[]{:S(2)}) async-start(), calls=%async_computation.5 | async-start | bytes 1572864 | tf_op jit(solution)/shard_map/all_gather | solution.py:27
  8.3 1.8 copy-start.12
  8.3 2.0 copy-start.6
  10.6 1.2 copy-start.7
  11.8 6.2 %copy-start.3 = (f32[64,8,8,128]{3,2,1,0:T(8,128)}, f32[64,8,8,128]{3,2,1,0:T(8,128)S(1)}, u32[]{:S(2)}) copy-start(f32[64,8,8,128]{3,2,1,0:T(8,128)S(1)} %copy.60) | copy-start | bytes 6291460
  14.0 4.0 %copy-start.5 = (f32[64,8,8,128]{3,2,1,0:T(8,128)S(1)}, f32[64,8,8,128]{3,2,1,0:T(8,128)}, u32[]{:S(2)}) copy-start(f32[64,8,8,128]{3,2,1,0:T(8,128)} %copy.58) | copy-start | bytes 6291460
  67.5 0.8 copy-start.2
  67.5 22.2 %copy-start.11 = (bf16[64,1024]{1,0:T(8,128)(2,1)S(1)}, bf16[64,1024]{1,0:T(8,128)(2,1)}, u32[]{:S(2)}) copy-start(bf16[64,1024]{1,0:T(8,128)(2,1)} %param.19) | copy-start | bytes 393220
  68.3 55.4 %all-gather.11.cloned.1.call-start = ((), (), s32[]{:S(2)}) async-start(), calls=%async_computation | async-start | bytes 2621440 | tf_op jit(solution)/shard_map/all_gather | solution.py:27
  89.7 90.6 %all-gather.17.cloned.1.call-start = ((), (), s32[]{:S(2)}) async-start(), calls=%async_computation.3 | async-start | bytes 4718592 | tf_op jit(solution)/shard_map/all_gather | solution.py:46
  100.8 134.7 %all-gather.13.cloned.1.call-start = ((), (), s32[]{:S(2)}) async-start(), calls=%async_computation.1 | async-start | bytes 4718592 | tf_op jit(solution)/shard_map/all_gather | solution.py:27
  126.3 135.5 %all-gather.19.cloned.1.call-start = ((), (), s32[]{:S(2)}) async-start(), calls=%async_computation.4 | async-start | bytes 12582912 | tf_op jit(solution)/shard_map/all_gather | solution.py:46
  180.3 19.7 %copy-start.13 = (f32[128]{0:T(128)S(1)}, f32[128]{0:T(128)}, u32[]{:S(2)}) copy-start(f32[128]{0:T(128)} %param.18) | copy-start | bytes 1540
  180.3 20.6 %copy-start.4 = (f32[64,8,8,128]{3,2,1,0:T(8,128)S(1)}, f32[64,8,8,128]{3,2,1,0:T(8,128)}, u32[]{:S(2)}) copy-start(f32[64,8,8,128]{3,2,1,0:T(8,128)} %copy-done.3) | copy-start | bytes 6291460
  180.4 134.4 %all-gather.15.cloned.1.call-start = ((), (), s32[]{:S(2)}) async-start(), calls=%async_computation.2 | async-start | bytes 5242880 | tf_op jit(solution)/shard_map/all_gather | solution.py:154
  200.9 34.6 %copy-start.8 = (f32[16,128,128]{2,1,0:T(8,128)S(1)}, f32[16,128,128]{2,1,0:T(8,128)}, u32[]{:S(2)}) copy-start(f32[16,128,128]{2,1,0:T(8,128)} %all-gather.21.cloned.1.call-done) | copy-start | bytes 3145732
  245.0 1.2 copy-start.10
  314.7 16.1 %copy-start.9 = (bf16[512,1024]{1,0:T(8,128)(2,1)S(1)}, bf16[512,1024]{1,0:T(8,128)(2,1)}, u32[]{:S(2)}) copy-start(bf16[512,1024]{1,0:T(8,128)(2,1)} %param.21) | copy-start | bytes 3145732
  314.7 16.1 %dynamic-slice-start = ((f32[4096]{0:T(1024)}, s32[]{:T(128)}), f32[1024]{0:T(1024)S(1)}, s32[]{:S(2)}) async-start(f32[4096]{0:T(1024)} %param.20, s32[]{:T(128)} %select_n.164), calls=%async_computation.6 | async-start | bytes 8704 | tf_op jit(solution)/shard_map/dynamic_slice | solution.py:162
  314.7 17.5 %copy-start.1 = (f32[4096]{0:T(1024)S(1)}, f32[4096]{0:T(1024)}, u32[]{:S(2)}) copy-start(f32[4096]{0:T(1024)} %param.16) | copy-start | bytes 49156
Sparse Core Ops, SparseCore 0:
  68.5 18.8 all-gather.20
  89.9 33.8 all-gather.10
  125.5 54.8 all-gather.16
  182.0 53.4 all-gather.12
  237.2 24.6 all-gather.18
  263.5 51.1 all-gather.14
where the time goes:
time: 341 us; the launch traced here: 339 us
  waiting for transfers between devices  169 us (50%)
  blocking collectives  51.7 us (15%)
  matrix products  46 us (13%)
  local copies, waits for them, and re-layouts  34.6 us (10%)
  other arithmetic  23.3 us (7%)
  between operations  13.7 us (4%)
    all_gather x2, waiting for transfers between devices, gather_in_order(): tiles = lax.all_gather(tiles, axes[k], axis=0, tiled=True)  67.3 us
    all_gather x3, waiting for transfers between devices, carried_in(): pieces = jax.tree.map(lambda part: lax.all_gather(part, axis), so_far)  57.2 us
    all_gather x1, waiting for transfers between devices, per_device(): all_heads = lax.all_gather(mixed_rows, 'tp', axis=1, tiled=True)  44.5 us
    all_gather x3, blocking collectives, carried_in(): pieces = jax.tree.map(lambda part: lax.all_gather(part, axis), so_far)  34.1 us
    dynamic_slice x24, local copies, waits for them, and re-layouts, per_device(): lax.scan(step_forward, starting_state, (queries, to_blocks(keys_in), to_b...  17.5 us
    all_gather x1, blocking collectives, gather_in_order(): tiles = lax.all_gather(tiles, axes[k], axis=0, tiled=True)  11 us
    dot_general x8, matrix products, block_update(): jnp.einsum('hsd,hse->hde', keys_in * jnp.exp(ending - running), values_in...  9.25 us
    dot_general x1, matrix products, per_device(): jnp.dot(all_heads, whole_of(output_matrix, SP, (1, 0, 2), 0), preferred_e...  9.21 us
  transfers between devices with their start and end apart: 6, of which 6 were waited for; matrix products, arithmetic and copies ran while one was open for 9% of the time, Pallas kernels for 0%

commit v1 on v0

v1 whole, which is shorter than its diff:
```python
import jax
import jax.numpy as jnp
from jax import lax
from jax.experimental import pallas as pl
from jax.experimental.pallas import tpu as pltpu
from jax.sharding import Mesh
from jax.sharding import PartitionSpec as P

HEAD_DIM = 128
D = 4096
EPS = 1e-06
TOK = 512
HEADS = 8
CHUNK = 128
CHUNKS = TOK // CHUNK
COLS = HEADS * HEAD_DIM
NZ, NX, NC, NY = 8, 4, 2, 4
ROW = NX * NC
SP = ("z", "x", "c")
MESH = pl.DeviceIdType.MESH
F32 = jnp.float32
BF16 = jnp.bfloat16

NT = (((1,), (1,)), ((), ()))
TN = (((0,), (0,)), ((), ()))
NN = (((1,), (0,)), ((), ()))


def dot(a, b, dims=NN):
    return lax.dot_general(a, b, dims, preferred_element_type=F32)


def split2(v):
    hi = v.astype(BF16)
    return hi, (v - hi.astype(F32)).astype(BF16)


def split3(v):
    hi = v.astype(BF16)
    left = v - hi.astype(F32)
    mid = left.astype(BF16)
    return hi.astype(F32), mid.astype(F32), left - mid.astype(F32)


def log_rows(v):
    hi, mid, lo = split3(v)
    row = lax.broadcasted_iota(jnp.int32, (16, HEAD_DIM), 0)
    block = jnp.where(row == 0, hi, jnp.where(row == 1, mid, jnp.where(row == 2, lo, 0.0)))
    return block.astype(BF16)


def rows_log(block):
    return jnp.sum(block.astype(F32), axis=0, keepdims=True)


def kernel(
    q_hbm, f_hbm, v_hbm, g_hbm, w_hbm, res_hbm, gap_ref, surge_ref, hgain_ref, bgain_ref,
    out_ref,
    qb, fb, vb, gb, resb, wf, mix, ra, kt, qe, intra, gate, deltas, rows, tri, surge3,
    send1, recv1, prefix, plog, send2, recv2, send3, recv3, sq_send, sq_recv, acc,
    load_sem, s1, r1, s2, r2, s3, r3, ys, yr, yfs, yfr, wzs, wzr, wxs, wxr, wfs, wfr, wds, wdr, qs_, qr_,
):
    z, x, c, y = (lax.axis_index(n) for n in ("z", "x", "c", "y"))
    rank = x * NC + c

    def at_row(r):
        return (z, lax.div(r, NC), lax.rem(r, NC), y)

    def at_z(k):
        return (lax.rem(z + k + NZ, NZ), x, c, y)

    def at_x(k):
        return (z, lax.rem(x + k + NX, NX), c, y)

    def at_y(k):
        return (z, x, c, lax.rem(y + k + NY, NY))

    sibling = (z, x, 1 - c, y)

    def remote(src, dst, send, recv, to):
        return pltpu.make_async_remote_copy(
            src_ref=src, dst_ref=dst, send_sem=send, recv_sem=recv, device_id=to, device_id_type=MESH
        )

    started = []

    def go(*args):
        copy = remote(*args)
        copy.start()
        started.append(copy)
        return copy

    piece = (z * NX + x, c)
    loads = []
    for k, (src, dst) in enumerate(
        ((w_hbm, wf.at[piece[0], piece[1]]), (f_hbm, fb), (v_hbm, vb), (q_hbm, qb), (g_hbm, gb), (res_hbm, resb))
    ):
        copy = pltpu.make_async_copy(src, dst, load_sem.at[k])
        copy.start()
        loads.append(copy)
    barrier = pltpu.get_barrier_semaphore()
    peers = [at_row(lax.rem(rank + d, ROW)) for d in range(1, ROW)]
    peers += [at_z(d) for d in range(1, NZ)]
    peers += [at_y(d) for d in range(1, NY)]
    for peer in peers:
        pl.semaphore_signal(barrier, inc=1, device_id=peer, device_id_type=MESH)

    lane = lax.broadcasted_iota(jnp.int32, (CHUNK, 2 * CHUNK), 1)
    at = lax.broadcasted_iota(jnp.int32, (CHUNK, 2 * CHUNK), 0)
    tri[...] = jnp.where(lax.rem(lane, CHUNK) <= at, 1.0, 0.0).astype(BF16)
    hi, mid, lo = split3(surge_ref[...])
    surge3[...] = jnp.concatenate([hi, mid, lo, jnp.zeros_like(hi)], axis=0).astype(BF16)

    loads[0].wait()
    pl.semaphore_wait(barrier, len(peers))

    def w_piece(zz, xx, cc):
        return wf.at[lax.rem(zz + NZ, NZ) * NX + lax.rem(xx + NX, NX), cc]

    def w_up(step):
        return go(w_piece(z - step, x, c), w_piece(z - step, x, c), wzs.at[0, step], wzr.at[0, step], at_z(1))

    def w_down(step):
        return go(w_piece(z + step, x, c), w_piece(z + step, x, c), wzs.at[1, step], wzr.at[1, step], at_z(-1))

    w_z = [(w_up(0), w_down(0))]

    loads[1].wait()
    loads[2].wait()

    @pl.loop(0, HEADS)
    def _(h):
        cols = pl.ds(pl.multiple_of(h * HEAD_DIM, HEAD_DIM), HEAD_DIM)
        gap = gap_ref[y * HEADS + h]
        pick = lax.broadcasted_iota(jnp.int32, (32, HEAD_DIM), 0)
        pick = jnp.where(lax.rem(pick, HEADS) == h, 1.0, 0.0).astype(BF16)
        surge = dot(surge3[...], pick, TN)
        state = jnp.zeros((HEAD_DIM, HEAD_DIM), F32)
        whole = jnp.zeros((1, HEAD_DIM), F32)
        for n in range(CHUNKS):
            span = pl.ds(n * CHUNK, CHUNK)
            keys = gap / (1.0 + jnp.exp(fb[span, cols].astype(F32)))
            series = 1.0 / 8.0
            for term in range(7, 0, -1):
                series = 1.0 / term + keys * series
            decay = surge[n * CHUNK : (n + 1) * CHUNK] - keys * series
            high, low = split2(decay)
            running = dot(tri[...], jnp.concatenate([high, low], axis=0))
            anchor = running[CHUNK // 2 - 1 : CHUNK // 2]
            ending = running[CHUNK - 1 : CHUNK]
            above = running - anchor
            ra[span, cols] = above
            scaled = (keys * jnp.exp(-above)).astype(BF16)
            kt[span, cols] = scaled
            rows[h, n, 0:1] = anchor
            rows[h, n, 1:2] = ending
            delta = dot(vb[span, cols], scaled, TN) * jnp.exp(ending - anchor)
            deltas[h, n] = delta
            state = state * jnp.exp(ending) + delta
            whole = whole + ending
        send1[h, 0:HEAD_DIM] = state.astype(BF16)
        send1[h, HEAD_DIM:] = log_rows(whole)

    phase1 = []
    for d in range(1, ROW):
        t = lax.rem(rank + d, ROW)
        phase1.append(go(send1.at[t], recv1.at[d], s1.at[d], r1.at[d], at_row(t)))
    recv1[0] = send1[rank]

    w_z[0][0].wait_recv()
    w_z[0][1].wait_recv()
    w_z.append((w_up(1), w_down(1)))

    def scores_of(h):
        cols = pl.ds(pl.multiple_of(h * HEAD_DIM, HEAD_DIM), HEAD_DIM)
        gain = hgain_ref[...]
        r = lax.broadcasted_iota(jnp.int32, (CHUNK, CHUNK), 0)
        s = lax.broadcasted_iota(jnp.int32, (CHUNK, CHUNK), 1)
        for n in range(CHUNKS):
            span = pl.ds(n * CHUNK, CHUNK)
            v = qb[span, cols].astype(F32)
            queries = v / (1.0 + jnp.exp(-v)) * HEAD_DIM ** (-0.5) * jnp.exp(ra[span, cols])
            scores = dot(queries.astype(BF16), kt[span, cols], NT)
            scores = jnp.where(s <= r, scores, 0.0).astype(BF16)
            intra[span, cols] = dot(scores, vb[span, cols])
            qe[span, cols] = (queries * jnp.exp(rows[h, n, 0:1])).astype(BF16)
            v = gb[span, cols].astype(F32)
            gate[span, cols] = v / (1.0 + jnp.exp(-v)) * gain

    loads[3].wait()
    loads[4].wait()
    pl.loop(0, HEADS // 2)(scores_of)

    for copy in phase1:
        copy.wait_recv()
    total = jnp.zeros((HEAD_DIM, HEAD_DIM), F32)
    total_log = jnp.zeros((1, HEAD_DIM), F32)
    for k in range(ROW):
        slot = lax.rem(rank - k + ROW, ROW)
        prefix[k] = total
        plog[k] = total_log
        here = rows_log(recv1[slot, HEAD_DIM:])
        total = total * jnp.exp(here) + recv1[slot, 0:HEAD_DIM].astype(F32)
        total_log = total_log + here
    send2[0:HEAD_DIM] = total.astype(BF16)
    send2[HEAD_DIM:] = log_rows(total_log)

    phase2 = [go(send2, recv2.at[d], s2.at[d], r2.at[d], at_z(d)) for d in range(1, NZ)]

    w_z[1][0].wait_recv()
    w_z[1][1].wait_recv()
    w_z.append((w_up(2), w_down(2)))
    pl.loop(HEADS // 2, HEADS)(scores_of)
    w_z[2][0].wait_recv()
    w_z[2][1].wait_recv()
    w_z.append((w_up(3),))

    for copy in phase2:
        copy.wait_recv()
    carry = jnp.zeros((HEAD_DIM, HEAD_DIM), F32)
    for k in range(NZ - 1):
        slot = lax.max(lax.rem(z - k + NZ, NZ), 1)
        here = rows_log(recv2[slot, HEAD_DIM:])
        after = carry * jnp.exp(here) + recv2[slot, 0:HEAD_DIM].astype(F32)
        carry = jnp.where(k < z, after, carry)
    for d in range(ROW):
        t = lax.rem(rank + d, ROW)
        send3[d] = (prefix[t] + carry * jnp.exp(plog[t])).astype(BF16)

    phase3 = []
    for d in range(1, ROW):
        t = lax.rem(rank + d, ROW)
        phase3.append(go(send3.at[d], recv3.at[d], s3.at[d], r3.at[d], at_row(t)))
    recv3[0] = send3[0]

    w_z[3][0].wait_recv()
    offsets = (0, 1, -2, -1, 2, 3, 4, 5)
    places = [lax.rem(2 * y + o + NZ, NZ) for o in offsets]
    w_x = []
    for k, zz in enumerate(places):
        here = w_piece(zz, x, c)
        w_x.append((
            go(here, here, wxs.at[0, k], wxr.at[0, k], at_x(1)),
            go(here, here, wxs.at[1, k], wxr.at[1, k], at_x(-1)),
        ))

    for copy in phase3:
        copy.wait_recv()

    y_own = []
    for j in range(HEADS // 2):

        @pl.loop(0, 2)
        def _(i):
            h = 2 * j + i
            cols = pl.ds(pl.multiple_of(h * HEAD_DIM, HEAD_DIM), HEAD_DIM)
            half = pl.ds(pl.multiple_of(i * HEAD_DIM, HEAD_DIM), HEAD_DIM)
            state = recv3[lax.rem(rank - h + ROW, ROW)].astype(F32)
            for n in range(CHUNKS):
                span = pl.ds(n * CHUNK, CHUNK)
                heads = intra[span, cols] + dot(qe[span, cols], state.astype(BF16), NT)
                mean = jnp.sum(heads * heads, axis=1, keepdims=True) * (1.0 / HEAD_DIM)
                mix[0, j, span, half] = (heads * lax.rsqrt(mean + EPS) * gate[span, cols]).astype(BF16)
                if n < CHUNKS - 1:
                    state = state * jnp.exp(rows[h, n, 1:2]) + deltas[h, n]

        y_own.append((
            go(mix.at[0, j], mix.at[1, j], ys.at[0, j], yr.at[0, j], at_y(1)),
            go(mix.at[0, j], mix.at[2, j], ys.at[1, j], yr.at[1, j], at_y(-1)),
        ))

    w_fwd, w_core, y_fwd = [], [], []

    def w_forward(k):
        zz = places[k]
        up, down = w_x[k]
        up.wait_recv()
        down.wait_recv()
        if k % 2 == 0:
            there = w_piece(zz, x - 1, c)
            w_fwd.append(go(there, there, wfs.at[k], wfr.at[k], at_x(1)))
        else:
            there = w_piece(zz, x + 1, c)
            w_fwd.append(go(there, there, wfs.at[k], wfr.at[k], at_x(-1)))

    def w_swap(k):
        w_fwd[k].wait_recv()
        there = wf.at[pl.ds(places[k] * NX, NX), c]
        w_core.append(go(there, there, wds.at[k], wdr.at[k], sibling))

    def y_forward(j):
        up, down = y_own[j]
        up.wait_recv()
        down.wait_recv()
        if j % 2 == 0:
            y_fwd.append(go(mix.at[1, j], mix.at[3, j], yfs.at[j], yfr.at[j], at_y(1)))
        else:
            y_fwd.append(go(mix.at[2, j], mix.at[3, j], yfs.at[j], yfr.at[j], at_y(-1)))

    def multiply(slot, place, j, first=False):
        first_row = lax.rem(y + place + NY, NY) * (2 * HEADS // 2) + 2 * j

        @pl.loop(0, COLS // 256)
        def _(n):
            cols = pl.ds(pl.multiple_of(n * 256, 256), 256)
            weights = wf[pl.ds(first_row, 2), :, :, cols].reshape(256, 256)
            product = dot(mix[slot, j], weights)
            acc[:, cols] = product if first else acc[:, cols] + product

    for k in range(2):
        w_forward(k)
    for j in range(2):
        y_forward(j)
    for k in range(2, 4):
        w_forward(k)
    for j in range(2, 4):
        y_forward(j)
    for k in range(4, 8):
        w_forward(k)
    for k in range(8):
        w_swap(k)
    for k in range(2):
        w_core[k].wait_recv()
    for j in range(4):
        multiply(0, 0, j, j == 0)
    for k in range(2, 4):
        w_core[k].wait_recv()
    for j in range(4):
        multiply(1, -1, j)
    for k in range(4, 6):
        w_core[k].wait_recv()
    for j in range(4):
        multiply(2, 1, j)
    for k in range(6, 8):
        w_core[k].wait_recv()
    for j in range(4):
        y_fwd[j].wait_recv()
        multiply(3, 2, j)

    part = jnp.zeros((8, TOK), F32)
    ones = jnp.ones((8, 256), BF16)
    for n in range(COLS // 256):
        branch = acc[:, n * 256 : (n + 1) * 256].astype(BF16).astype(F32)
        high, low = split2(branch * branch)
        part = part + dot(ones, high, NT) + dot(ones, low, NT)
    sq_send[...] = part
    squares = [go(sq_send, sq_recv.at[d], qs_.at[d], qr_.at[d], at_y(d)) for d in range(1, NY)]
    for copy in squares:
        copy.wait_recv()
    for d in range(1, NY):
        part = part + sq_recv[d]
    scale = lax.rsqrt(part * (1.0 / D) + EPS)
    hi, mid, lo = split3(scale)
    parts = jnp.concatenate([hi, mid, lo, jnp.zeros_like(lo)], axis=0).astype(BF16)
    pick = lax.broadcasted_iota(jnp.int32, (32, HEAD_DIM), 0)
    pick = jnp.where(lax.rem(pick, 8) == 0, 1.0, 0.0).astype(BF16)
    column = dot(parts, pick, TN)
    loads[5].wait()

    for h in range(HEADS):
        cols = slice(h * HEAD_DIM, (h + 1) * HEAD_DIM)
        branch = acc[:, cols].astype(BF16).astype(F32)
        out_ref[:, cols] = (
            resb[:, cols].astype(F32) + branch * column * bgain_ref[y * HEADS + h]
        ).astype(BF16)

    for copy in started:
        copy.wait_send()


def per_device(q, f, v, g, gap, surge, hgain, w, bgain, res):
    any_ = pl.BlockSpec(memory_space=pl.ANY)
    vmem = pl.BlockSpec(memory_space=pltpu.VMEM)
    dma = pltpu.SemaphoreType.DMA
    block = (TOK, COLS)
    square = (HEAD_DIM, HEAD_DIM)
    message = (HEAD_DIM + 16, HEAD_DIM)
    scratch = [
        pltpu.VMEM(block, BF16),
        pltpu.VMEM(block, BF16),
        pltpu.VMEM(block, BF16),
        pltpu.VMEM(block, BF16),
        pltpu.VMEM(block, BF16),
        pltpu.VMEM((NZ * NX, NC, 64, COLS), BF16),
        pltpu.VMEM((NY, HEADS // 2, TOK, 256), BF16),
        pltpu.VMEM(block, F32),
        pltpu.VMEM(block, BF16),
        pltpu.VMEM(block, BF16),
        pltpu.VMEM(block, F32),
        pltpu.VMEM(block, F32),
        pltpu.VMEM((HEADS, CHUNKS) + square, F32),
        pltpu.VMEM((HEADS, CHUNKS, 8, HEAD_DIM), F32),
        pltpu.VMEM((CHUNK, 2 * CHUNK), BF16),
        pltpu.VMEM((32, TOK), BF16),
        pltpu.VMEM((ROW,) + message, BF16),
        pltpu.VMEM((ROW,) + message, BF16),
        pltpu.VMEM((ROW,) + square, F32),
        pltpu.VMEM((ROW, 1, HEAD_DIM), F32),
        pltpu.VMEM(message, BF16),
        pltpu.VMEM((NZ,) + message, BF16),
        pltpu.VMEM((ROW,) + square, BF16),
        pltpu.VMEM((ROW,) + square, BF16),
        pltpu.VMEM((8, TOK), F32),
        pltpu.VMEM((NY, 8, TOK), F32),
        pltpu.VMEM(block, F32),
        dma((6,)),
        dma((ROW,)), dma((ROW,)), dma((NZ,)), dma((NZ,)), dma((ROW,)), dma((ROW,)),
        dma((2, 4)), dma((2, 4)), dma((4,)), dma((4,)),
        dma((2, 4)), dma((2, 4)), dma((2, 8)), dma((2, 8)), dma((8,)), dma((8,)), dma((8,)), dma((8,)),
        dma((NY,)), dma((NY,)),
    ]
    return pl.pallas_call(
        kernel,
        out_shape=jax.ShapeDtypeStruct(block, BF16),
        in_specs=[any_] * 6 + [vmem] * 4,
        out_specs=vmem,
        scratch_shapes=scratch,
        compiler_params=pltpu.CompilerParams(
            collective_id=0, has_side_effects=True, vmem_limit_bytes=62 * 1024 * 1024
        ),
    )(
        q, f, v, g, w, res,
        gap.reshape(NY * HEADS, 1, HEAD_DIM), surge, hgain.reshape(1, HEAD_DIM),
        bgain.reshape(NY * HEADS, 1, HEAD_DIM),
    )


def solution(mesh):
    torus = Mesh(mesh.devices.reshape(NZ, NX, NC, NY), ("z", "x", "c", "y"))
    cut = P(SP, "y")
    in_specs = (cut, cut, cut, cut, P(), P("y", SP), P(), cut, P(), cut)
    return jax.shard_map(per_device, mesh=torus, in_specs=in_specs, out_specs=cut, check_vma=False)
```

time: 341 us -> 100 us (0.29)
  waiting for transfers between devices: 169 us -> 0 us
  Pallas kernels: 0 us -> 96.4 us
  blocking collectives: 51.7 us -> 0 us
  matrix products: 46 us -> 0 us
  local copies, waits for them, and re-layouts: 34.6 us -> 2.26 us
  other arithmetic: 23.3 us -> 0 us
  between operations: 13.7 us -> 0.01 us
    all_gather x6 -> x0, waiting for transfers between devices: 169 us -> none  [the longest x2 67.3 us: gather_in_order(): tiles = lax.all_gather(tiles, axes[k], axis=0, tiled=True)]
    pallas_call x0 -> x1, Pallas kernels: none -> 96.4 us  [per_device(): pl.pallas_call(kernel, out_shape=jax.ShapeDtypeStruct(block, BF16), in_sp...]
    dot_general x34 -> x0, matrix products: 46 us -> none  [the longest x8 9.25 us: block_update(): jnp.einsum('hsd,hse->hde', keys_in * jnp.exp(ending - running), values_in...]
    all_gather x4 -> x0, blocking collectives: 45.1 us -> none  [the longest x3 34.1 us: carried_in(): pieces = jax.tree.map(lambda part: lax.all_gather(part, axis), so_far)]
    dynamic_slice x26 -> x0, local copies, waits for them, and re-layouts: 17.5 us -> none  [the longest x24 17.5 us: per_device(): lax.scan(step_forward, starting_state, (queries, to_blocks(keys_in), to_b...]
    transpose x3 -> x0, local copies, waits for them, and re-layouts: 11.1 us -> none  [the longest x1 8.41 us: gather_in_order(): tiles.transpose(*turned, *range(len(turns), tiles.ndim))]
    psum x1 -> x0, blocking collectives: 6.59 us -> none  [per_device(): squares = lax.psum(jnp.sum(branch * branch, axis=1), 'tp')]
    add x2 -> x0, other arithmetic: 4.93 us -> none  [combine(): return (earlier[0] * later[0], later[0][:, :, None] * earlier[1] + later[1])]
  transfers between devices with their start and end apart: 6 -> 0, of which waited for: 6 -> 0; matrix products, arithmetic and copies ran while one was open for 9% -> 0% of each run, Pallas kernels for 0% -> 0%
where the time goes in v1:
time: 100 us; the launch traced here: 98.7 us
  Pallas kernels  96.4 us (96%)
  local copies, waits for them, and re-layouts  2.26 us (2%)
    pallas_call x1, Pallas kernels, per_device(): pl.pallas_call(kernel, out_shape=jax.ShapeDtypeStruct(block, BF16), in_sp...  96.4 us
    unnamed x1, local copies, waits for them, and re-layouts  2.26 us

profile of v1, /device:TPU:1, one launch (start us, length us, event | category | flops | bytes accessed | tf_op | source)
XLA Modules:
  0.0 98.7 jit_solution(13268556372151159004)
XLA Ops:
  0.0 96.4 %shard_map.100 = bf16[512,1024]{1,0:T(8,128)(2,1)} custom-call(bf16[512,1024]{1,0:T(8,128)(2,1)} %q_hbm.1, bf16[512,1024]{1,0:T(8,128)(2,1)} %f_hbm.1, bf16[512,1024]{1,0:T(8,128)(2,1)} %v_hbm.1, bf16[512,1024]{1,0:T(8,128)(2,1)} %g_hbm.1, bf16[64,1024]{1,0:T(8,128)(2,1)} %w_hbm.1, bf16[512,1024]{1,0:T(8,128)(2,1)} %res_hbm.1, f32[32,1,128]{2,1,0:T(1,128)} %bitcast.3, ...), custom_call_target="tpu_custom_call" | custom-call | tf_op jit(solution)/shard_map/pallas_call | solution.py:412
  96.4 2.3 %copy.12 = bf16[512,1024]{1,0:T(8,128)(2,1)} copy(bf16[512,1024]{1,0:T(8,128)(2,1)} %shard_map.100) | data formatting | bytes 2097152

commit v2 on v1

v2 whole, which is shorter than its diff:
```python
import jax
import jax.numpy as jnp
from jax import lax
from jax.experimental import pallas as pl
from jax.experimental.pallas import tpu as pltpu
from jax.sharding import Mesh
from jax.sharding import PartitionSpec as P

HEAD_DIM = 128
D = 4096
EPS = 1e-06
LOG2E = 1.4426950408889634
TOK = 512
HEADS = 8
CHUNK = 128
CHUNKS = TOK // CHUNK
COLS = HEADS * HEAD_DIM
NZ, NX, NC, NY = 8, 4, 2, 4
ROW = NX * NC
GROUPS = 4
GROUP_HEADS = HEADS // GROUPS
SPLIT = ROW // GROUP_HEADS
PART = HEAD_DIM // SPLIT
PAIR = 2 * HEAD_DIM
VMEM_LIMIT = 65_980_000
SP = ("z", "x", "c")
MESH = pl.DeviceIdType.MESH
F32 = jnp.float32
BF16 = jnp.bfloat16

NT = (((1,), (1,)), ((), ()))
TN = (((0,), (0,)), ((), ()))
NN = (((1,), (0,)), ((), ()))

LOG_SERIES = (1.442695046784621, 0.7213445806373628, 0.48113117086413326, 0.3542908416742433, 0.3582091924805078)


def dot(a, b, dims=NN):
    return lax.dot_general(a, b, dims, preferred_element_type=F32)


def split2(v):
    hi = v.astype(BF16)
    return hi, (v - hi.astype(F32)).astype(BF16)


def split3(v):
    hi = v.astype(BF16).astype(F32)
    left = v - hi
    mid = left.astype(BF16).astype(F32)
    return hi, mid, left - mid


def log_rows(v):
    hi, mid, lo = split3(v)
    row = lax.broadcasted_iota(jnp.int32, (16, HEAD_DIM), 0)
    block = jnp.where(row == 0, hi, jnp.where(row == 1, mid, jnp.where(row == 2, lo, 0.0)))
    return block.astype(BF16)


def rows_log(block):
    return jnp.sum(block.astype(F32), axis=0, keepdims=True)


def kernel(
    q_hbm, f_hbm, v_hbm, g_hbm, w_hbm, res_hbm, gap_ref, surge_ref, hgain_ref, bgain_ref,
    out_ref,
    qb, fb, vb, gb, branch_buf, resb, wf, mix, ra, kt, qe, intra, gate, deltas, rows, tri, surge3,
    send1, recv1, prefix, plog, send2, recv2, send3, recv3, sq_send, sq_recv, acc,
    load_sem, s1, r1, s2, r2, s3, r3, ys, yr, yfs, yfr,
    azs, azr, bxs, bxr, bfs, bfr, axs, axr, afs, afr, bzs, bzr, wds, wdr, qs_, qr_,
):
    z, x, c, y = (lax.axis_index(n) for n in ("z", "x", "c", "y"))
    rank = x * NC + c

    def at_row(r):
        return (z, lax.div(r, NC), lax.rem(r, NC), y)

    def wrap_z(k):
        return lax.rem(z + k + NZ, NZ)

    def wrap_x(k):
        return lax.rem(x + k + NX, NX)

    def at_z(k):
        return (wrap_z(k), x, c, y)

    def at_x(k):
        return (z, wrap_x(k), c, y)

    def at_y(k):
        return (z, x, c, lax.rem(y + k + NY, NY))

    sibling = (z, x, 1 - c, y)
    started = []

    def go(src, dst, send, recv, to):
        copy = pltpu.make_async_remote_copy(
            src_ref=src, dst_ref=dst, send_sem=send, recv_sem=recv, device_id=to, device_id_type=MESH
        )
        copy.start()
        started.append(copy)
        return copy

    EARLY, LATE = pl.ds(0, COLS // 2), pl.ds(COLS // 2, COLS // 2)
    loads = []
    for k, (src, dst) in enumerate(
        (
            (f_hbm.at[:, EARLY], fb.at[:, EARLY]), (v_hbm.at[:, EARLY], vb.at[:, EARLY]), (w_hbm, wf.at[z, x, c]),
            (f_hbm.at[:, LATE], fb.at[:, LATE]), (v_hbm.at[:, LATE], vb.at[:, LATE]), (q_hbm, qb), (g_hbm, gb),
            (res_hbm, resb),
        )
    ):
        copy = pltpu.make_async_copy(src, dst, load_sem.at[k])
        copy.start()
        loads.append(copy)
    load_f, load_v, load_w, *loads_late, load_q, load_g, load_res = loads
    barrier = pltpu.get_barrier_semaphore()
    peers = [at_row(lax.rem(rank + d, ROW)) for d in range(1, ROW)]
    peers += [at_z(d) for d in range(1, NZ)]
    peers += [at_y(d) for d in range(1, NY)]
    for peer in peers:
        pl.semaphore_signal(barrier, inc=1, device_id=peer, device_id_type=MESH)

    lane = lax.broadcasted_iota(jnp.int32, (CHUNK, 2 * CHUNK), 1)
    at = lax.broadcasted_iota(jnp.int32, (CHUNK, 2 * CHUNK), 0)
    tri[...] = jnp.where(lax.rem(lane, CHUNK) <= at, 1.0, 0.0).astype(BF16)
    hi, mid, lo = split3(surge_ref[...] * LOG2E)
    surge3[...] = jnp.concatenate([hi, mid, lo, jnp.zeros_like(hi)], axis=0).astype(BF16)
    load_f.wait()
    load_v.wait()

    def states_of(p):
        cols = pl.ds(pl.multiple_of(p * PAIR, PAIR), PAIR)
        gap = gap_ref[y * (HEADS // 2) + p] * 0.5
        pick = lax.broadcasted_iota(jnp.int32, (32, PAIR), 0)
        head = 2 * p + lax.div(lax.broadcasted_iota(jnp.int32, (32, PAIR), 1), HEAD_DIM)
        pick = jnp.where(lax.rem(pick, HEADS) == head, 1.0, 0.0).astype(BF16)
        surge = dot(surge3[...], pick, TN)
        state = [jnp.zeros((HEAD_DIM, HEAD_DIM), F32)] * 2
        whole = jnp.zeros((1, PAIR), F32)
        for n in range(CHUNKS):
            span = pl.ds(n * CHUNK, CHUNK)
            keys = gap - gap * jnp.tanh(fb[span, cols].astype(F32) * 0.5)
            series = LOG_SERIES[-1]
            for term in LOG_SERIES[-2::-1]:
                series = term + keys * series
            decay = surge[n * CHUNK : (n + 1) * CHUNK] - keys * series
            high, low = split2(decay)
            running = dot(tri[...], jnp.concatenate([high, low], axis=0))
            anchor = running[CHUNK // 2 - 1 : CHUNK // 2]
            ending = running[CHUNK - 1 : CHUNK]
            above = running - anchor
            ra[span, cols] = above
            scaled = (keys * jnp.exp2(-above)).astype(BF16)
            kt[span, cols] = scaled
            shrink = jnp.exp2(ending)
            tail = jnp.exp2(ending - anchor)
            rows[p, n, 0:1] = jnp.exp2(anchor)
            rows[p, n, 1:2] = shrink
            values = vb[span, cols]
            for i in range(2):
                half = slice(i * HEAD_DIM, (i + 1) * HEAD_DIM)
                delta = dot(values[:, half], scaled[:, half], TN) * tail[:, half]
                deltas[2 * p + i, n] = delta
                state[i] = state[i] * shrink[:, half] + delta
            whole = whole + ending
        for i in range(2):
            block = state[i].astype(BF16)
            logs = log_rows(whole[:, i * HEAD_DIM : (i + 1) * HEAD_DIM])
            for e in range(SPLIT):
                send1[p, SPLIT * i + e, 0:PART] = block[e * PART : (e + 1) * PART]
                send1[p, SPLIT * i + e, PART:] = logs

    def send_states(g):
        copies = []
        for d in range(1, ROW):
            t = lax.rem(rank + d, ROW)
            copies.append(go(send1.at[g, t], recv1.at[g, d], s1.at[g, d], r1.at[g, d], at_row(t)))
        recv1[g, 0] = send1[g, rank]
        return copies

    def send_totals(g, arriving):
        for copy in arriving:
            copy.wait_recv()
        total = jnp.zeros((PART, HEAD_DIM), F32)
        total_log = jnp.zeros((1, HEAD_DIM), F32)
        for k in range(ROW):
            slot = lax.rem(rank - k + ROW, ROW)
            prefix[g, k] = total
            plog[g, k] = total_log
            here = rows_log(recv1[g, slot, PART:])
            total = total * jnp.exp2(here) + recv1[g, slot, 0:PART].astype(F32)
            total_log = total_log + here
        send2[g, 0:PART] = total.astype(BF16)
        send2[g, PART:] = log_rows(total_log)
        return [go(send2.at[g], recv2.at[g, d], s2.at[g, d], r2.at[g, d], at_z(d)) for d in range(1, NZ)]

    def send_carried(g, arriving):
        for copy in arriving:
            copy.wait_recv()
        carry = jnp.zeros((PART, HEAD_DIM), F32)
        for k in range(NZ - 1):
            slot = lax.max(lax.rem(z - k + NZ, NZ), 1)
            here = rows_log(recv2[g, slot, PART:])
            after = carry * jnp.exp2(here) + recv2[g, slot, 0:PART].astype(F32)
            carry = jnp.where(k < z, after, carry)
        copies = []
        for d in range(ROW):
            t = lax.rem(rank + d, ROW)
            send3[g, d] = (prefix[g, t] + carry * jnp.exp2(plog[g, t])).astype(BF16)
            if d > 0:
                copies.append(go(send3.at[g, d], recv3.at[g, d], s3.at[g, d], r3.at[g, d], at_row(t)))
        recv3[g, 0] = send3[g, 0]
        return copies

    def scores_of(p):
        gain = hgain_ref[...] * 0.5
        r = lax.broadcasted_iota(jnp.int32, (CHUNK, CHUNK), 0)
        s = lax.broadcasted_iota(jnp.int32, (CHUNK, CHUNK), 1)
        for i in range(2):
            cols = pl.ds(pl.multiple_of(p * PAIR + i * HEAD_DIM, HEAD_DIM), HEAD_DIM)
            for n in range(CHUNKS):
                span = pl.ds(n * CHUNK, CHUNK)
                v = qb[span, cols].astype(F32)
                h = v * (0.5 * HEAD_DIM ** (-0.5))
                queries = (h + h * jnp.tanh(v * 0.5)) * jnp.exp2(ra[span, cols])
                scores = dot(queries.astype(BF16), kt[span, cols], NT)
                scores = jnp.where(s <= r, scores, 0.0).astype(BF16)
                intra[span, cols] = dot(scores, vb[span, cols])
                qe[span, cols] = (queries * rows[p, n, 0:1, i * HEAD_DIM : (i + 1) * HEAD_DIM]).astype(BF16)
                v = gb[span, cols].astype(F32)
                h = v * gain
                gate[span, cols] = h + h * jnp.tanh(v * 0.5)

    y_own = []

    def finish(j):
        for i in range(2):
            h = 2 * j + i
            cols = pl.ds(h * HEAD_DIM, HEAD_DIM)
            slots = [lax.rem(rank - (SPLIT * i + e) + ROW, ROW) for e in range(SPLIT)]
            state = jnp.concatenate([recv3[j, slot].astype(F32) for slot in slots], axis=0)
            for n in range(CHUNKS):
                span = pl.ds(n * CHUNK, CHUNK)
                heads = intra[span, cols] + dot(qe[span, cols], state.astype(BF16), NT)
                mean = jnp.sum(heads * heads, axis=1, keepdims=True) * (1.0 / HEAD_DIM)
                mix[0, span, cols] = (heads * lax.rsqrt(mean + EPS) * gate[span, cols]).astype(BF16)
                if n < CHUNKS - 1:
                    state = state * rows[j, n, 1:2, i * HEAD_DIM : (i + 1) * HEAD_DIM] + deltas[h, n]
        part = pl.ds(j * PAIR, PAIR)
        y_own.append((
            go(mix.at[0, :, part], mix.at[1, :, part], ys.at[0, j], yr.at[0, j], at_y(1)),
            go(mix.at[0, :, part], mix.at[2, :, part], ys.at[1, j], yr.at[1, j], at_y(-1)),
        ))

    A, B = pl.ds(0, 32), pl.ds(32, 32)

    OFFSETS = (0, -1, 1, -2, 2, -3, 3, 4)

    def a_send(k, offset, d):
        ref = wf.at[wrap_z(offset), x, c, A]
        return go(ref, ref, azs.at[k], azr.at[k], at_z(d))

    away = 2 - 4 * c

    def a_out(k):
        ref = wf.at[wrap_z(OFFSETS[k]), x, c, A]
        return [go(ref, ref, axs.at[i, k], axr.at[i, k], at_x(d)) for i, d in enumerate((1, -1))]

    def a_forward(k):
        wait_both(a_x[k])
        d = 1 if k % 2 == 0 else -1
        ref = wf.at[wrap_z(OFFSETS[k]), wrap_x(-d), c, A]
        return go(ref, ref, afs.at[k], afr.at[k], at_x(d))

    def b_go(way, step, m):
        ref = wf.at[wrap_z(step if way else -step), pl.ds(2 * m, 2), c, B]
        return go(ref, ref, bzs.at[way, step, m], bzr.at[way, step, m], at_z(-1 if way else 1))

    def b_send(step):
        return [[b_go(way, step, m) for way in range(2)] for m in range(2)]

    def b_next(step):
        b_ring.append([])
        for m in range(2):
            wait_both(b_ring[step - 1][m])
            b_ring[step].append([b_go(way, step, m) for way in range(2) if step < 3 or way == m])

    def wait_both(copies):
        for copy in copies:
            copy.wait_recv()

    swaps = []

    def swap(ref):
        k = len(swaps)
        swaps.append(go(ref, ref, wds.at[k], wdr.at[k], sibling))

    pl.loop(0, 2)(states_of)
    pl.semaphore_wait(barrier, len(peers))
    arriving1 = [send_states(0), send_states(1)]
    load_w.wait()
    a_z = [a_send(0, 0, 1), a_send(1, 0, -1), a_send(2, 0, 2), a_send(3, 0, -2)]
    own_b = wf.at[z, x, c, B]
    b_x = (go(own_b, own_b, bxs.at[0], bxr.at[0], at_x(1)), go(own_b, own_b, bxs.at[1], bxr.at[1], at_x(-1)))
    loads_late[0].wait()
    loads_late[1].wait()
    states_of(2)
    arriving1.append(send_states(2))
    states_of(3)
    arriving1.append(send_states(3))
    load_q.wait()
    load_g.wait()
    scores_of(0)
    arriving2 = [send_totals(0, arriving1[0])]
    arriving2.append(send_totals(1, arriving1[1]))
    scores_of(1)
    arriving2.append(send_totals(2, arriving1[2]))
    arriving2.append(send_totals(3, arriving1[3]))
    scores_of(2)
    arriving3 = [send_carried(0, arriving2[0])]
    arriving3.append(send_carried(1, arriving2[1]))
    wait_both(b_x)
    ref = wf.at[z, wrap_x(-1), c, pl.ds(32, 16)]
    b_f = [go(ref, ref, bfs.at[0], bfr.at[0], at_x(1))]
    ref = wf.at[z, wrap_x(1), c, pl.ds(48, 16)]
    b_f.append(go(ref, ref, bfs.at[1], bfr.at[1], at_x(-1)))
    wait_both(a_z[0:4])
    a_z += [a_send(4, -2, 1), a_send(5, 2, -1), a_send(6, -away, away)]
    a_x = [a_out(k) for k in range(3)]
    scores_of(3)
    wait_both(arriving3[0])
    finish(0)
    wait_both(b_f)
    b_ring = [b_send(0)]
    wait_both(arriving3[1])
    finish(1)
    arriving3.append(send_carried(2, arriving2[2]))
    arriving3.append(send_carried(3, arriving2[3]))
    a_x += [a_out(k) for k in range(3, 5)]
    a_f = [a_forward(k) for k in range(3)]
    wait_both(arriving3[2])
    finish(2)
    wait_both(arriving3[3])
    finish(3)

    wait_both(a_z[4:7])
    a_x += [a_out(k) for k in range(5, 8)]
    b_next(1)
    for k in (0, -1, 1):
        swap(wf.at[wrap_z(k), :, c, B])
    a_f += [a_forward(k) for k in range(3, 5)]
    b_next(2)
    for k in (-2, 2):
        swap(wf.at[wrap_z(k), :, c, B])
    a_f += [a_forward(k) for k in range(5, 8)]
    y_fwd = []

    HALVES = (pl.ds(0, TOK // 2), pl.ds(TOK // 2, TOK // 2))

    def y_forward(j):
        wait_both(y_own[j])
        part = pl.ds(j * PAIR, PAIR)
        d = 1 if j % 2 == 0 else -1
        source = 1 if d == 1 else 2
        y_fwd.append([
            go(mix.at[source, half, part], mix.at[3, half, part], yfs.at[j, m], yfr.at[j, m], at_y(d))
            for m, half in enumerate(HALVES)
        ])

    y_forward(0)
    y_forward(1)
    b_next(3)
    for k in (-3, 3):
        swap(wf.at[wrap_z(k), :, c, B])
    wait_both(a_f)
    for m in range(2):
        swap(wf.at[pl.ds(4 * m, 4), :, c, A])
    y_forward(2)
    y_forward(3)
    for m in range(2):
        wait_both(b_ring[3][m])
    swap(wf.at[wrap_z(4), :, c, B])
    wait_both(swaps)

    def multiply(slot, place, m=None, rows_=pl.ds(0, TOK)):
        first = 2 * lax.rem(y + place + NY, NY)
        depth = COLS if m is None else COLS // 2
        left = pl.ds(0 if m is None else m * depth, depth)

        @pl.loop(0, COLS // 256)
        def _(n):
            cols = pl.ds(pl.multiple_of(n * 256, 256), 256)
            if m is None:
                weights = wf[pl.ds(first, 2), :, :, :, cols].reshape(depth, 256)
            else:
                weights = wf[first + m, :, :, :, cols].reshape(depth, 256)
            product = dot(mix[slot, rows_, left], weights)
            acc[rows_, cols] = product if slot == 0 else acc[rows_, cols] + product

    for slot, place in ((0, 0), (1, -1), (2, 1)):
        multiply(slot, place)
    wait_both(y_fwd[0] + y_fwd[1])
    multiply(3, 2, 0)

    load_res.wait()

    def squares_of(m):
        rows_ = HALVES[m]
        wait_both((y_fwd[2][m], y_fwd[3][m]))
        multiply(3, 2, 1, rows_)
        part = jnp.zeros((8, TOK // 2), F32)
        ones = jnp.ones((8, 256), BF16)
        for n in range(COLS // 256):
            cols = slice(n * 256, (n + 1) * 256)
            branch = acc[rows_, cols].astype(BF16)
            branch_buf[rows_, cols] = branch
            branch = branch.astype(F32)
            high, low = split2(branch * branch)
            part = part + dot(ones, high, NT) + dot(ones, low, NT)
        sq_send[m] = part
        return [go(sq_send.at[m], sq_recv.at[m, d], qs_.at[m, d], qr_.at[m, d], at_y(d)) for d in range(1, NY)]

    def write(m, squares):
        rows_ = HALVES[m]
        wait_both(squares)
        part = sq_send[m]
        for d in range(1, NY):
            part = part + sq_recv[m, d]
        scale = lax.rsqrt(part * (1.0 / D) + EPS)
        hi, mid, lo = split3(scale)
        parts = jnp.concatenate([hi, mid, lo, jnp.zeros_like(lo)], axis=0).astype(BF16)
        pick = lax.broadcasted_iota(jnp.int32, (32, HEAD_DIM), 0)
        pick = jnp.where(lax.rem(pick, 8) == 0, 1.0, 0.0).astype(BF16)
        column = dot(parts, pick, TN)
        for h in range(HEADS):
            cols = slice(h * HEAD_DIM, (h + 1) * HEAD_DIM)
            out_ref[rows_, cols] = (
                resb[rows_, cols].astype(F32) + branch_buf[rows_, cols].astype(F32) * column * bgain_ref[y * HEADS + h]
            ).astype(BF16)

    squares = [squares_of(0)]
    squares.append(squares_of(1))
    write(0, squares[0])
    write(1, squares[1])
    for copy in started:
        copy.wait_send()


def per_device(q, f, v, g, gap, surge, hgain, w, bgain, res):
    any_ = pl.BlockSpec(memory_space=pltpu.HBM)
    vmem = pl.BlockSpec(memory_space=pltpu.VMEM)
    dma = pltpu.SemaphoreType.DMA
    block = (TOK, COLS)
    state = (PART, HEAD_DIM)
    message = (PART + 16, HEAD_DIM)
    scratch = [
        pltpu.VMEM(block, BF16),
        pltpu.VMEM(block, BF16),
        pltpu.VMEM(block, BF16),
        pltpu.VMEM(block, BF16),
        pltpu.VMEM(block, BF16),
        pltpu.VMEM(block, BF16),
        pltpu.VMEM((NZ, NX, NC, 64, COLS), BF16),
        pltpu.VMEM((NY,) + block, BF16),
        pltpu.VMEM(block, F32),
        pltpu.VMEM(block, BF16),
        pltpu.VMEM(block, BF16),
        pltpu.VMEM(block, F32),
        pltpu.VMEM(block, F32),
        pltpu.VMEM((HEADS, CHUNKS, HEAD_DIM, HEAD_DIM), F32),
        pltpu.VMEM((HEADS // 2, CHUNKS, 8, PAIR), F32),
        pltpu.VMEM((CHUNK, 2 * CHUNK), BF16),
        pltpu.VMEM((32, TOK), BF16),
        pltpu.VMEM((GROUPS, ROW) + message, BF16),
        pltpu.VMEM((GROUPS, ROW) + message, BF16),
        pltpu.VMEM((GROUPS, ROW) + state, F32),
        pltpu.VMEM((GROUPS, ROW, 1, HEAD_DIM), F32),
        pltpu.VMEM((GROUPS,) + message, BF16),
        pltpu.VMEM((GROUPS, NZ) + message, BF16),
        pltpu.VMEM((GROUPS, ROW) + state, BF16),
        pltpu.VMEM((GROUPS, ROW) + state, BF16),
        pltpu.VMEM((2, 8, TOK // 2), F32),
        pltpu.VMEM((2, NY, 8, TOK // 2), F32),
        pltpu.VMEM(block, F32),
        dma((8,)),
        dma((GROUPS, ROW)), dma((GROUPS, ROW)), dma((GROUPS, NZ)), dma((GROUPS, NZ)),
        dma((GROUPS, ROW)), dma((GROUPS, ROW)),
        dma((2, 4)), dma((2, 4)), dma((4, 2)), dma((4, 2)),
        dma((7,)), dma((7,)), dma((2,)), dma((2,)), dma((2,)), dma((2,)),
        dma((2, 8)), dma((2, 8)), dma((8,)), dma((8,)), dma((2, 4, 2)), dma((2, 4, 2)), dma((10,)), dma((10,)),
        dma((2, NY)), dma((2, NY)),
    ]
    return pl.pallas_call(
        kernel,
        out_shape=pltpu.VMEM(block, BF16),
        in_specs=[any_] * 6 + [vmem] * 4,
        out_specs=vmem,
        scratch_shapes=scratch,
        compiler_params=pltpu.CompilerParams(
            collective_id=0, has_side_effects=True, vmem_limit_bytes=VMEM_LIMIT
        ),
    )(
        q, f, v, g, w, res,
        gap.reshape(NY * HEADS // 2, 1, PAIR), surge, hgain.reshape(1, HEAD_DIM),
        bgain.reshape(NY * HEADS, 1, HEAD_DIM),
    )


def solution(mesh):
    torus = Mesh(mesh.devices.reshape(NZ, NX, NC, NY), ("z", "x", "c", "y"))
    cut = P(SP, "y")
    in_specs = (cut, cut, cut, cut, P(), P("y", SP), P(), cut, P(), cut)
    return jax.shard_map(per_device, mesh=torus, in_specs=in_specs, out_specs=cut, check_vma=False)
```

time: 100 us -> 71.8 us (0.72); the launches traced: 98.7 us -> 71.5 us
  Pallas kernels: 96.4 us -> 70.5 us
  local copies, waits for them, and re-layouts: 2.26 us -> 0.97 us
    pallas_call x1, Pallas kernels: 96.4 us -> 70.5 us  [per_device(): pl.pallas_call(kernel, out_shape=pltpu.VMEM(block, BF16), in_specs=[any_]...]
    unnamed x1, local copies, waits for them, and re-layouts: 2.26 us -> 0.97 us
where the time goes in v2:
time: 71.8 us; the launch traced here: 71.5 us
  Pallas kernels  70.5 us (98%)
  local copies, waits for them, and re-layouts  0.97 us (1%)
    pallas_call x1, Pallas kernels, per_device(): pl.pallas_call(kernel, out_shape=pltpu.VMEM(block, BF16), in_specs=[any_]...  70.5 us

profile of v2, /device:TPU:1, one launch (start us, length us, event | category | flops | bytes accessed | tf_op | source)
XLA Modules:
  0.0 71.5 jit_solution(17056449184233016100)
XLA Ops:
  0.0 70.5 %shard_map.100 = bf16[512,1024]{1,0:T(8,128)(2,1)S(1)} custom-call(bf16[512,1024]{1,0:T(8,128)(2,1)} %q_hbm.1, bf16[512,1024]{1,0:T(8,128)(2,1)} %f_hbm.1, bf16[512,1024]{1,0:T(8,128)(2,1)} %v_hbm.1, bf16[512,1024]{1,0:T(8,128)(2,1)} %g_hbm.1, bf16[64,1024]{1,0:T(8,128)(2,1)} %w_hbm.1, bf16[512,1024]{1,0:T(8,128)(2,1)} %res_hbm.1, f32[16,1,256]{2,1,0:T(1,128)} %bitcast.3, ...), custom_call_target="tpu_custom_call" | custom-call | tf_op jit(solution)/shard_map/pallas_call | solution.py:495
  70.5 1.0 %copy.12 = bf16[512,1024]{1,0:T(8,128)(2,1)} copy(bf16[512,1024]{1,0:T(8,128)(2,1)S(1)} %shard_map.100) | data formatting | bytes 2097152

commit v3 on v2

--- a/solution.py
+++ b/solution.py
@@ -63,12 +63,12 @@
 
 
 def kernel(
-    q_hbm, f_hbm, v_hbm, g_hbm, w_hbm, res_hbm, gap_ref, surge_ref, hgain_ref, bgain_ref,
+    q_hbm, f_hbm, v_hbm, g_hbm, w_hbm, res_hbm, gap_hbm, surge_hbm, hgain_hbm, bgain_hbm,
     out_ref,
-    qb, fb, vb, gb, branch_buf, resb, wf, mix, ra, kt, qe, intra, gate, deltas, rows, tri, surge3,
+    qb, fb, vb, gb, branch_buf, resb, gap_ref, surge_ref, hgain_ref, bgain_ref, wf, mix,
+    ra, kt, qe, intra, gate, deltas, rows, tri, surge3,
     send1, recv1, prefix, plog, send2, recv2, send3, recv3, sq_send, sq_recv, acc,
-    load_sem, s1, r1, s2, r2, s3, r3, ys, yr, yfs, yfr,
-    azs, azr, bxs, bxr, bfs, bfr, axs, axr, afs, afr, bzs, bzr, wds, wdr, qs_, qr_,
+    load_sem, sent, r1, r2, r3, yr, yfr, ar, br, wdr, qr_,
 ):
     z, x, c, y = (lax.axis_index(n) for n in ("z", "x", "c", "y"))
     rank = x * NC + c
@@ -92,29 +92,19 @@
         return (z, x, c, lax.rem(y + k + NY, NY))
 
     sibling = (z, x, 1 - c, y)
-    started = []
+
+    def done(sem, view):
+        pltpu.make_async_copy(view, view, sem).wait()
+
+    PHASE1, PHASE2, PHASE3, OVER_Y, A_Z, A_X, B_X, B_Z, CORES, SQUARES = (sent.at[k] for k in range(10))
 
     def go(src, dst, send, recv, to):
         copy = pltpu.make_async_remote_copy(
             src_ref=src, dst_ref=dst, send_sem=send, recv_sem=recv, device_id=to, device_id_type=MESH
         )
         copy.start()
-        started.append(copy)
-        return copy
 
     EARLY, LATE = pl.ds(0, COLS // 2), pl.ds(COLS // 2, COLS // 2)
-    loads = []
-    for k, (src, dst) in enumerate(
-        (
-            (f_hbm.at[:, EARLY], fb.at[:, EARLY]), (v_hbm.at[:, EARLY], vb.at[:, EARLY]), (w_hbm, wf.at[z, x, c]),
-            (f_hbm.at[:, LATE], fb.at[:, LATE]), (v_hbm.at[:, LATE], vb.at[:, LATE]), (q_hbm, qb), (g_hbm, gb),
-            (res_hbm, resb),
-        )
-    ):
-        copy = pltpu.make_async_copy(src, dst, load_sem.at[k])
-        copy.start()
-        loads.append(copy)
-    load_f, load_v, load_w, *loads_late, load_q, load_g, load_res = loads
     barrier = pltpu.get_barrier_semaphore()
     peers = [at_row(lax.rem(rank + d, ROW)) for d in range(1, ROW)]
     peers += [at_z(d) for d in range(1, NZ)]
@@ -122,13 +112,27 @@
     for peer in peers:
         pl.semaphore_signal(barrier, inc=1, device_id=peer, device_id_type=MESH)
 
+    def load(k, *pairs):
+        for src, dst in pairs:
+            pltpu.make_async_copy(src, dst, load_sem.at[k]).start()
+
+    load(0, (f_hbm.at[:, EARLY], fb.at[:, EARLY]), (v_hbm.at[:, EARLY], vb.at[:, EARLY]))
+    load(1, (surge_hbm, surge_ref))
+    load(2, (gap_hbm, gap_ref))
+    load(3, (w_hbm, wf.at[z, x, c]))
+    load(4, (f_hbm.at[:, LATE], fb.at[:, LATE]), (v_hbm.at[:, LATE], vb.at[:, LATE]))
+    load(5, (q_hbm, qb), (g_hbm, gb))
+    load(6, (hgain_hbm, hgain_ref))
+    load(7, (bgain_hbm, bgain_ref))
+    load(8, (res_hbm, resb))
     lane = lax.broadcasted_iota(jnp.int32, (CHUNK, 2 * CHUNK), 1)
     at = lax.broadcasted_iota(jnp.int32, (CHUNK, 2 * CHUNK), 0)
     tri[...] = jnp.where(lax.rem(lane, CHUNK) <= at, 1.0, 0.0).astype(BF16)
+    done(load_sem.at[1], surge_ref)
     hi, mid, lo = split3(surge_ref[...] * LOG2E)
     surge3[...] = jnp.concatenate([hi, mid, lo, jnp.zeros_like(hi)], axis=0).astype(BF16)
-    load_f.wait()
-    load_v.wait()
+    done(load_sem.at[2], gap_ref)
+    done(load_sem.at[0], fb)
 
     def states_of(p):
         cols = pl.ds(pl.multiple_of(p * PAIR, PAIR), PAIR)
@@ -173,16 +177,13 @@
                 send1[p, SPLIT * i + e, PART:] = logs
 
     def send_states(g):
-        copies = []
         for d in range(1, ROW):
             t = lax.rem(rank + d, ROW)
-            copies.append(go(send1.at[g, t], recv1.at[g, d], s1.at[g, d], r1.at[g, d], at_row(t)))
+            go(send1.at[g, t], recv1.at[g, d], PHASE1, r1.at[g], at_row(t))
         recv1[g, 0] = send1[g, rank]
-        return copies
-
-    def send_totals(g, arriving):
-        for copy in arriving:
-            copy.wait_recv()
+
+    def send_totals(g):
+        done(r1.at[g], recv1.at[g, pl.ds(1, ROW - 1)])
         total = jnp.zeros((PART, HEAD_DIM), F32)
         total_log = jnp.zeros((1, HEAD_DIM), F32)
         for k in range(ROW):
@@ -194,25 +195,23 @@
             total_log = total_log + here
         send2[g, 0:PART] = total.astype(BF16)
         send2[g, PART:] = log_rows(total_log)
-        return [go(send2.at[g], recv2.at[g, d], s2.at[g, d], r2.at[g, d], at_z(d)) for d in range(1, NZ)]
-
-    def send_carried(g, arriving):
-        for copy in arriving:
-            copy.wait_recv()
+        for d in range(1, NZ):
+            go(send2.at[g], recv2.at[g, d], PHASE2, r2.at[g], at_z(d))
+
+    def send_carried(g):
+        done(r2.at[g], recv2.at[g, pl.ds(1, NZ - 1)])
         carry = jnp.zeros((PART, HEAD_DIM), F32)
         for k in range(NZ - 1):
             slot = lax.max(lax.rem(z - k + NZ, NZ), 1)
             here = rows_log(recv2[g, slot, PART:])
             after = carry * jnp.exp2(here) + recv2[g, slot, 0:PART].astype(F32)
             carry = jnp.where(k < z, after, carry)
-        copies = []
         for d in range(ROW):
             t = lax.rem(rank + d, ROW)
             send3[g, d] = (prefix[g, t] + carry * jnp.exp2(plog[g, t])).astype(BF16)
             if d > 0:
-                copies.append(go(send3.at[g, d], recv3.at[g, d], s3.at[g, d], r3.at[g, d], at_row(t)))
+                go(send3.at[g, d], recv3.at[g, d], PHASE3, r3.at[g], at_row(t))
         recv3[g, 0] = send3[g, 0]
-        return copies
 
     def scores_of(p):
         gain = hgain_ref[...] * 0.5
@@ -233,9 +232,8 @@
                 h = v * gain
                 gate[span, cols] = h + h * jnp.tanh(v * 0.5)
 
-    y_own = []
-
     def finish(j):
+        done(r3.at[j], recv3.at[j, pl.ds(1, ROW - 1)])
         for i in range(2):
             h = 2 * j + i
             cols = pl.ds(h * HEAD_DIM, HEAD_DIM)
@@ -249,149 +247,140 @@
                 if n < CHUNKS - 1:
                     state = state * rows[j, n, 1:2, i * HEAD_DIM : (i + 1) * HEAD_DIM] + deltas[h, n]
         part = pl.ds(j * PAIR, PAIR)
-        y_own.append((
-            go(mix.at[0, :, part], mix.at[1, :, part], ys.at[0, j], yr.at[0, j], at_y(1)),
-            go(mix.at[0, :, part], mix.at[2, :, part], ys.at[1, j], yr.at[1, j], at_y(-1)),
-        ))
+        go(mix.at[0, :, part], mix.at[1, :, part], OVER_Y, yr.at[j], at_y(1))
+        go(mix.at[0, :, part], mix.at[2, :, part], OVER_Y, yr.at[j], at_y(-1))
 
     A, B = pl.ds(0, 32), pl.ds(32, 32)
 
     OFFSETS = (0, -1, 1, -2, 2, -3, 3, 4)
+    BATCH = (0, 0, 0, 1, 1, 2, 2, 2)
+    away = 2 - 4 * c
 
     def a_send(k, offset, d):
         ref = wf.at[wrap_z(offset), x, c, A]
-        return go(ref, ref, azs.at[k], azr.at[k], at_z(d))
-
-    away = 2 - 4 * c
+        go(ref, ref, A_Z, ar.at[k], at_z(d))
 
     def a_out(k):
         ref = wf.at[wrap_z(OFFSETS[k]), x, c, A]
-        return [go(ref, ref, axs.at[i, k], axr.at[i, k], at_x(d)) for i, d in enumerate((1, -1))]
-
-    def a_forward(k):
-        wait_both(a_x[k])
-        d = 1 if k % 2 == 0 else -1
-        ref = wf.at[wrap_z(OFFSETS[k]), wrap_x(-d), c, A]
-        return go(ref, ref, afs.at[k], afr.at[k], at_x(d))
+        for d in (1, -1):
+            go(ref, ref, A_X, ar.at[2 + BATCH[k]], at_x(d))
+
+    def a_forward(batch):
+        ks = [k for k in range(NZ) if BATCH[k] == batch]
+        done(ar.at[2 + batch], wf.at[pl.ds(0, len(ks)), pl.ds(0, 2), 0, A])
+        for k in ks:
+            d = 1 if k % 2 == 0 else -1
+            ref = wf.at[wrap_z(OFFSETS[k]), wrap_x(-d), c, A]
+            go(ref, ref, A_X, ar.at[5], at_x(d))
 
     def b_go(way, step, m):
         ref = wf.at[wrap_z(step if way else -step), pl.ds(2 * m, 2), c, B]
-        return go(ref, ref, bzs.at[way, step, m], bzr.at[way, step, m], at_z(-1 if way else 1))
+        go(ref, ref, B_Z, br.at[2 * step + m if step < 3 else 6], at_z(-1 if way else 1))
 
     def b_send(step):
-        return [[b_go(way, step, m) for way in range(2)] for m in range(2)]
-
-    def b_next(step):
-        b_ring.append([])
         for m in range(2):
-            wait_both(b_ring[step - 1][m])
-            b_ring[step].append([b_go(way, step, m) for way in range(2) if step < 3 or way == m])
-
-    def wait_both(copies):
-        for copy in copies:
-            copy.wait_recv()
-
-    swaps = []
+            if step > 0:
+                done(br.at[2 * step - 2 + m], wf.at[pl.ds(0, 2), pl.ds(0, 2), 0, B])
+            for way in range(2):
+                if step < 3 or way == m:
+                    b_go(way, step, m)
 
     def swap(ref):
-        k = len(swaps)
-        swaps.append(go(ref, ref, wds.at[k], wdr.at[k], sibling))
+        go(ref, ref, CORES, wdr.at[0], sibling)
 
     pl.loop(0, 2)(states_of)
     pl.semaphore_wait(barrier, len(peers))
-    arriving1 = [send_states(0), send_states(1)]
-    load_w.wait()
-    a_z = [a_send(0, 0, 1), a_send(1, 0, -1), a_send(2, 0, 2), a_send(3, 0, -2)]
+    send_states(0)
+    send_states(1)
+    done(load_sem.at[3], w_hbm)
+    for k, d in enumerate((1, -1, 2, -2)):
+        a_send(0, 0, d)
     own_b = wf.at[z, x, c, B]
-    b_x = (go(own_b, own_b, bxs.at[0], bxr.at[0], at_x(1)), go(own_b, own_b, bxs.at[1], bxr.at[1], at_x(-1)))
-    loads_late[0].wait()
-    loads_late[1].wait()
+    go(own_b, own_b, B_X, br.at[7], at_x(1))
+    go(own_b, own_b, B_X, br.at[7], at_x(-1))
+    done(load_sem.at[4], fb)
     states_of(2)
-    arriving1.append(send_states(2))
+    send_states(2)
     states_of(3)
-    arriving1.append(send_states(3))
-    load_q.wait()
-    load_g.wait()
+    send_states(3)
+    done(load_sem.at[5], mix.at[pl.ds(0, 2)])
+    done(load_sem.at[6], hgain_ref)
     scores_of(0)
-    arriving2 = [send_totals(0, arriving1[0])]
-    arriving2.append(send_totals(1, arriving1[1]))
+    send_totals(0)
+    send_totals(1)
     scores_of(1)
-    arriving2.append(send_totals(2, arriving1[2]))
-    arriving2.append(send_totals(3, arriving1[3]))
+    send_totals(2)
+    send_totals(3)
     scores_of(2)
-    arriving3 = [send_carried(0, arriving2[0])]
-    arriving3.append(send_carried(1, arriving2[1]))
-    wait_both(b_x)
+    send_carried(0)
+    send_carried(1)
+    done(br.at[7], wf.at[pl.ds(0, 2), 0, 0, B])
     ref = wf.at[z, wrap_x(-1), c, pl.ds(32, 16)]
-    b_f = [go(ref, ref, bfs.at[0], bfr.at[0], at_x(1))]
+    go(ref, ref, B_X, br.at[8], at_x(1))
     ref = wf.at[z, wrap_x(1), c, pl.ds(48, 16)]
-    b_f.append(go(ref, ref, bfs.at[1], bfr.at[1], at_x(-1)))
-    wait_both(a_z[0:4])
-    a_z += [a_send(4, -2, 1), a_send(5, 2, -1), a_send(6, -away, away)]
-    a_x = [a_out(k) for k in range(3)]
+    go(ref, ref, B_X, br.at[8], at_x(-1))
+    done(ar.at[0], wf.at[pl.ds(0, 4), 0, 0, A])
+    a_send(1, -2, 1)
+    a_send(1, 2, -1)
+    a_send(1, -away, away)
+    for k in range(3):
+        a_out(k)
     scores_of(3)
-    wait_both(arriving3[0])
     finish(0)
-    wait_both(b_f)
-    b_ring = [b_send(0)]
-    wait_both(arriving3[1])
+    done(br.at[8], wf.at[0, 0, 0, pl.ds(0, 32)])
+    b_send(0)
     finish(1)
-    arriving3.append(send_carried(2, arriving2[2]))
-    arriving3.append(send_carried(3, arriving2[3]))
-    a_x += [a_out(k) for k in range(3, 5)]
-    a_f = [a_forward(k) for k in range(3)]
-    wait_both(arriving3[2])
+    send_carried(2)
+    send_carried(3)
+    for k in range(3, 5):
+        a_out(k)
+    a_forward(0)
     finish(2)
-    wait_both(arriving3[3])
     finish(3)
 
-    wait_both(a_z[4:7])
-    a_x += [a_out(k) for k in range(5, 8)]
-    b_next(1)
+    done(ar.at[1], wf.at[pl.ds(0, 3), 0, 0, A])
+    for k in range(5, 8):
+        a_out(k)
+    b_send(1)
     for k in (0, -1, 1):
         swap(wf.at[wrap_z(k), :, c, B])
-    a_f += [a_forward(k) for k in range(3, 5)]
-    b_next(2)
+    a_forward(1)
+    b_send(2)
     for k in (-2, 2):
         swap(wf.at[wrap_z(k), :, c, B])
-    a_f += [a_forward(k) for k in range(5, 8)]
-    y_fwd = []
-
+    a_forward(2)
     HALVES = (pl.ds(0, TOK // 2), pl.ds(TOK // 2, TOK // 2))
 
     def y_forward(j):
-        wait_both(y_own[j])
         part = pl.ds(j * PAIR, PAIR)
+        done(yr.at[j], mix.at[pl.ds(1, 2), :, part])
         d = 1 if j % 2 == 0 else -1
         source = 1 if d == 1 else 2
-        y_fwd.append([
-            go(mix.at[source, half, part], mix.at[3, half, part], yfs.at[j, m], yfr.at[j, m], at_y(d))
-            for m, half in enumerate(HALVES)
-        ])
+        for m, half in enumerate(HALVES):
+            sem = yfr.at[0 if j < 2 else 1 + m]
+            go(mix.at[source, half, part], mix.at[3, half, part], OVER_Y, sem, at_y(d))
 
     y_forward(0)
     y_forward(1)
-    b_next(3)
+    b_send(3)
     for k in (-3, 3):
         swap(wf.at[wrap_z(k), :, c, B])
-    wait_both(a_f)
+    done(ar.at[5], wf.at[:, 0, 0, A])
     for m in range(2):
         swap(wf.at[pl.ds(4 * m, 4), :, c, A])
     y_forward(2)
     y_forward(3)
-    for m in range(2):
-        wait_both(b_ring[3][m])
+    done(br.at[6], wf.at[pl.ds(0, 2), pl.ds(0, 2), 0, B])
     swap(wf.at[wrap_z(4), :, c, B])
-    wait_both(swaps)
+    done(wdr.at[0], wf.at[:, :, 0])
 
     def multiply(slot, place, m=None, rows_=pl.ds(0, TOK)):
         first = 2 * lax.rem(y + place + NY, NY)
         depth = COLS if m is None else COLS // 2
         left = pl.ds(0 if m is None else m * depth, depth)
 
-        @pl.loop(0, COLS // 256)
-        def _(n):
-            cols = pl.ds(pl.multiple_of(n * 256, 256), 256)
+        for n in range(COLS // 256):
+            cols = pl.ds(n * 256, 256)
             if m is None:
                 weights = wf[pl.ds(first, 2), :, :, :, cols].reshape(depth, 256)
             else:
@@ -401,14 +390,15 @@
 
     for slot, place in ((0, 0), (1, -1), (2, 1)):
         multiply(slot, place)
-    wait_both(y_fwd[0] + y_fwd[1])
+    done(yfr.at[0], mix.at[3, :, pl.ds(0, COLS // 2)])
     multiply(3, 2, 0)
 
-    load_res.wait()
+    done(load_sem.at[7], bgain_ref)
+    done(load_sem.at[8], resb)
 
     def squares_of(m):
         rows_ = HALVES[m]
-        wait_both((y_fwd[2][m], y_fwd[3][m]))
+        done(yfr.at[1 + m], mix.at[3, rows_, pl.ds(COLS // 2, COLS // 2)])
         multiply(3, 2, 1, rows_)
         part = jnp.zeros((8, TOK // 2), F32)
         ones = jnp.ones((8, 256), BF16)
@@ -420,11 +410,12 @@
             high, low = split2(branch * branch)
             part = part + dot(ones, high, NT) + dot(ones, low, NT)
         sq_send[m] = part
-        return [go(sq_send.at[m], sq_recv.at[m, d], qs_.at[m, d], qr_.at[m, d], at_y(d)) for d in range(1, NY)]
-
-    def write(m, squares):
+        for d in range(1, NY):
+            go(sq_send.at[m], sq_recv.at[m, d], SQUARES, qr_.at[m], at_y(d))
+
+    def write(m):
         rows_ = HALVES[m]
-        wait_both(squares)
+        done(qr_.at[m], sq_recv.at[m, pl.ds(1, NY - 1)])
         part = sq_send[m]
         for d in range(1, NY):
             part = part + sq_recv[m, d]
@@ -440,12 +431,20 @@
                 resb[rows_, cols].astype(F32) + branch_buf[rows_, cols].astype(F32) * column * bgain_ref[y * HEADS + h]
             ).astype(BF16)
 
-    squares = [squares_of(0)]
-    squares.append(squares_of(1))
-    write(0, squares[0])
-    write(1, squares[1])
-    for copy in started:
-        copy.wait_send()
+    squares_of(0)
+    squares_of(1)
+    write(0)
+    write(1)
+    done(PHASE1, recv1.at[:, pl.ds(1, ROW - 1)])
+    done(PHASE2, recv2.at[:, pl.ds(1, NZ - 1)])
+    done(PHASE3, recv3.at[:, pl.ds(1, ROW - 1)])
+    done(OVER_Y, mix.at[pl.ds(1, 3)])
+    done(A_Z, wf.at[pl.ds(0, 7), 0, 0, A])
+    done(A_X, wf.at[:, pl.ds(0, 3), 0, A])
+    done(B_X, wf.at[pl.ds(0, 3), 0, 0, A])
+    done(B_Z, wf.at[pl.ds(0, 7), :, 0, B])
+    done(CORES, wf.at[:, :, 0])
+    done(SQUARES, sq_recv.at[:, pl.ds(1, NY - 1)])
 
 
 def per_device(q, f, v, g, gap, surge, hgain, w, bgain, res):
@@ -462,6 +461,10 @@
         pltpu.VMEM(block, BF16),
         pltpu.VMEM(block, BF16),
         pltpu.VMEM(block, BF16),
+        pltpu.VMEM((NY * HEADS // 2, 1, PAIR), F32),
+        pltpu.VMEM((HEADS, TOK), F32),
+        pltpu.VMEM((1, HEAD_DIM), F32),
+        pltpu.VMEM((NY * HEADS, 1, HEAD_DIM), F32),
         pltpu.VMEM((NZ, NX, NC, 64, COLS), BF16),
         pltpu.VMEM((NY,) + block, BF16),
         pltpu.VMEM(block, F32),
@@ -484,18 +487,14 @@
         pltpu.VMEM((2, 8, TOK // 2), F32),
         pltpu.VMEM((2, NY, 8, TOK // 2), F32),
         pltpu.VMEM(block, F32),
-        dma((8,)),
-        dma((GROUPS, ROW)), dma((GROUPS, ROW)), dma((GROUPS, NZ)), dma((GROUPS, NZ)),
-        dma((GROUPS, ROW)), dma((GROUPS, ROW)),
-        dma((2, 4)), dma((2, 4)), dma((4, 2)), dma((4, 2)),
-        dma((7,)), dma((7,)), dma((2,)), dma((2,)), dma((2,)), dma((2,)),
-        dma((2, 8)), dma((2, 8)), dma((8,)), dma((8,)), dma((2, 4, 2)), dma((2, 4, 2)), dma((10,)), dma((10,)),
-        dma((2, NY)), dma((2, NY)),
+        dma((9,)),
+        dma((10,)),
+        dma((GROUPS,)), dma((GROUPS,)), dma((GROUPS,)), dma((4,)), dma((3,)), dma((6,)), dma((9,)), dma((1,)), dma((2,)),
     ]
     return pl.pallas_call(
         kernel,
         out_shape=pltpu.VMEM(block, BF16),
-        in_specs=[any_] * 6 + [vmem] * 4,
+        in_specs=[any_] * 10,
         out_specs=vmem,
         scratch_shapes=scratch,
         compiler_params=pltpu.CompilerParams(

time: 71.8 us -> 67.2 us (0.936)
  Pallas kernels: 70.5 us -> 66.1 us
    pallas_call x1, Pallas kernels: 70.5 us -> 66.1 us  [per_device(): pl.pallas_call(kernel, out_shape=pltpu.VMEM(block, BF16), in_specs=[any_]...]
where the time goes in v3:
time: 67.2 us; the launch traced here: 67.1 us
  Pallas kernels  66.1 us (98%)
  local copies, waits for them, and re-layouts  0.97 us (1%)
    pallas_call x1, Pallas kernels, per_device(): pl.pallas_call(kernel, out_shape=pltpu.VMEM(block, BF16), in_specs=[any_]...  66.1 us

profile of v3, /device:TPU:1, one launch (start us, length us, event | category | flops | bytes accessed | tf_op | source)
XLA Modules:
  0.0 67.1 jit_solution(13098481525338702077)
XLA Ops:
  0.0 66.1 %shard_map.100 = bf16[512,1024]{1,0:T(8,128)(2,1)S(1)} custom-call(bf16[512,1024]{1,0:T(8,128)(2,1)} %q_hbm.1, bf16[512,1024]{1,0:T(8,128)(2,1)} %f_hbm.1, bf16[512,1024]{1,0:T(8,128)(2,1)} %v_hbm.1, bf16[512,1024]{1,0:T(8,128)(2,1)} %g_hbm.1, bf16[64,1024]{1,0:T(8,128)(2,1)} %w_hbm.1, bf16[512,1024]{1,0:T(8,128)(2,1)} %res_hbm.1, f32[16,1,256]{2,1,0:T(1,128)} %bitcast.3, ...), custom_call_target="tpu_custom_call" | custom-call | tf_op jit(solution)/shard_map/pallas_call | solution.py:494
  66.1 1.0 %copy.12 = bf16[512,1024]{1,0:T(8,128)(2,1)} copy(bf16[512,1024]{1,0:T(8,128)(2,1)S(1)} %shard_map.100) | data formatting | bytes 2097152
